TPU v7x, 32 devices: a whole 2x2x4 slice. The times are simulated.
32 devices in a mesh: grp: 2 (over y), kv: 4 (over z), tp: 4 (over x, core).
Axes of the slice: x: 2, y: 2, z: 4, core: 2. Of those that a mesh axis runs over, the one named last changes fastest.
Arguments:
- residual: bfloat16 [32, 4096], P('grp', ('kv', 'tp')), parts along dimension 0, may hold values from -11 to 11
- cache_keys: bfloat16 [32, 4096, 8, 128], P('grp', 'kv', 'tp'), parts along dimension 0, may hold values from -210 to 210
- cache_values: bfloat16 [32, 4096, 8, 128], P('grp', 'kv', 'tp'), parts along dimension 0, may hold values from -6 to 6
- norm_gain: bfloat16 [4096], P('kv'), may hold values from 0.099609375 to 1.8984375
- query_weight: bfloat16 [4096, 2048], P('kv', 'tp'), may hold values from -0.09375 to 0.09375
- key_weight: bfloat16 [4096, 1024], P('kv', 'tp'), may hold values from -0.25 to 0.25
- value_weight: bfloat16 [4096, 1024], P('kv', 'tp'), may hold values from -0.375 to 0.375
- head_lambda: float32 [16], P('tp'), may hold values from 0.3 to 0.8
- head_gain: bfloat16 [128], replicated, may hold values from 0.099609375 to 1.8984375
- out_weight: bfloat16 [2048, 4096], P('tp', 'kv'), may hold values from -0.1875 to 0.1875
- mixer_gain: bfloat16 [4096], P('kv'), may hold values from 0.099609375 to 1.8984375
- up_weight: bfloat16 [4096, 16384], P('kv', 'tp'), may hold values from -0.09375 to 0.09375
- down_weight: bfloat16 [16384, 4096], P('tp', 'kv'), may hold values from -0.0625 to 0.0625
Outputs:
- updated: bfloat16 [32, 4096], P('grp', ('kv', 'tp')), parts along dimension 0
There are 2 independent parts, one for each index of `grp`. A program takes and returns all parts, laid end to end along the dimension named above; an argument that names none is the same for every part. Nothing has to cross between parts.
All inputs are finite; a program needn't handle non-finite values.
Results may differ from a plain program's by a relative error of at most 0.018.
Values may be sent and summed in bfloat16 or wider, within the bound.
A program may use at most 128 MiB of HBM per device.

v0:
```python
import jax
import jax.numpy as jnp
from jax import lax
from jax.sharding import PartitionSpec as P

D = 4096
HEADS = 16
KV_HEADS = 8
HALF = 64
VDIM = 128
EPS = 1e-06


def joined(shard, axis, combine):
    everything = jax.tree.map(lambda part: lax.all_gather(part, axis), shard)
    first = jax.tree.map(lambda part: part[0], everything)

    def step(k, so_far):
        return combine(so_far, jax.tree.map(lambda part: part[k], everything))

    return lax.fori_loop(1, lax.axis_size(axis), step, first)


def combine(first, second):
    top = jnp.maximum(first[0], second[0])
    left = jnp.exp(first[0] - top)
    right = jnp.exp(second[0] - top)
    return (
        top,
        first[1] * left + second[1] * right,
        first[2] * left[..., None] + second[2] * right[..., None],
    )


def body(
    residual,
    cache_keys,
    cache_values,
    norm_gain,
    query_weight,
    key_weight,
    value_weight,
    head_lambda,
    head_gain,
    out_weight,
    mixer_gain,
    up_weight,
    down_weight,
):
    f32 = jnp.float32
    bf16 = jnp.bfloat16
    rows = residual.shape[0]
    kv_local = cache_keys.shape[2]
    group = HEADS // KV_HEADS
    scale = 1.0 / HALF**0.5
    block = lax.all_gather(residual, "tp", axis=1, tiled=True).astype(f32)
    scaled = (block * norm_gain.astype(f32)).astype(bf16)
    q_part = jnp.dot(scaled, query_weight, preferred_element_type=f32)
    k_part = jnp.dot(scaled, key_weight, preferred_element_type=f32)
    v_part = jnp.dot(scaled, value_weight, preferred_element_type=f32)
    sq_part = jnp.sum(block * block, axis=1)
    q_sum, k_sum, v_sum, sq_sum = lax.psum((q_part, k_part, v_part, sq_part), "kv")
    inv_rms = lax.rsqrt(sq_sum / D + EPS)[:, None]
    query = (inv_rms * q_sum).astype(bf16).reshape(rows, kv_local, group, 2, HALF)
    new_key = (inv_rms * k_sum).astype(bf16).reshape(rows, kv_local, 2, HALF)
    new_value = (inv_rms * v_sum).astype(bf16).reshape(rows, kv_local, VDIM)
    positions = cache_keys.shape[1]
    keys = cache_keys.reshape(rows, positions, kv_local, 2, HALF)
    scores = jnp.einsum("bkgch,bpkch->bkgcp", query, keys, preferred_element_type=f32) * scale
    local_top = jnp.max(scores, axis=4)
    expo = jnp.exp(scores - local_top[..., None])
    local_total = jnp.sum(expo, axis=4)
    local_weighted = jnp.einsum(
        "bkgcp,bpkv->bkgcv", expo.astype(bf16), cache_values, preferred_element_type=f32
    )
    cache_top, total, weighted = joined((local_top, local_total, local_weighted), "kv", combine)
    own = jnp.einsum("bkgch,bkch->bkgc", query, new_key, preferred_element_type=f32) * scale
    top = jnp.maximum(cache_top, own)
    old_part = jnp.exp(cache_top - top)
    own_part = jnp.exp(own - top)
    numer = (
        weighted * old_part[..., None]
        + own_part[..., None] * new_value.astype(f32)[:, :, None, None, :]
    )
    attended = numer / (total * old_part + own_part)[..., None]
    lambdas = head_lambda.reshape(kv_local, group)[None, :, :, None]
    diff = attended[:, :, :, 0] - lambdas * attended[:, :, :, 1]
    normed = (
        diff * lax.rsqrt(jnp.mean(diff * diff, axis=3, keepdims=True) + EPS) * head_gain.astype(f32)
    )
    heads_out = normed.astype(bf16).reshape(rows, kv_local * group * VDIM)
    projected = jnp.dot(heads_out, out_weight, preferred_element_type=f32)
    mixed = (
        residual.astype(f32) + lax.psum_scatter(projected, "tp", scatter_dimension=1, tiled=True)
    ).astype(bf16)
    mixed_block = lax.all_gather(mixed, "tp", axis=1, tiled=True).astype(f32)
    scaled2 = (mixed_block * mixer_gain.astype(f32)).astype(bf16)
    up_part = jnp.dot(scaled2, up_weight, preferred_element_type=f32)
    sq_mixed = jnp.sum(mixed_block * mixed_block, axis=1)
    up_share = lax.psum_scatter(up_part, "kv", scatter_dimension=1, tiled=True)
    sq_total = lax.psum(sq_mixed, "kv")
    inv_rms2 = lax.rsqrt(sq_total / D + EPS)[:, None]
    share = jnp.square(jnp.maximum(inv_rms2 * up_share, 0.0)).astype(bf16)
    hidden = lax.all_gather(share, "kv", axis=1, tiled=True)
    down_part = jnp.dot(hidden, down_weight, preferred_element_type=f32)
    return (
        mixed.astype(f32) + lax.psum_scatter(down_part, "tp", scatter_dimension=1, tiled=True)
    ).astype(bf16)


def solution(mesh):
    in_specs = (
        P("grp", ("kv", "tp")),
        P("grp", "kv", "tp", None),
        P("grp", "kv", "tp", None),
        P("kv"),
        P("kv", "tp"),
        P("kv", "tp"),
        P("kv", "tp"),
        P("tp"),
        P(),
        P("tp", "kv"),
        P("kv"),
        P("kv", "tp"),
        P("tp", "kv"),
    )
    out_specs = P("grp", ("kv", "tp"))
    return jax.shard_map(body, mesh=mesh, in_specs=in_specs, out_specs=out_specs, check_vma=False)
```

profile of v0, /device:TPU:0, one launch (start us, length us, event | category | flops | bytes accessed | tf_op | source)
XLA Modules:
  0.0 212.5 jit_solution(997170010051651746)
XLA Ops:
  6.5 0.8 convert_element_type.64
  7.3 6.4 %all_gather.27 = bf16[16,1024]{1,0:T(8,128)(2,1)S(1)} all-gather(bf16[16,256]{1,0:T(8,128)(2,1)} %param.15), channel_id=1, replica_groups=mesh['grp'=2,'kv'=4,'tp'=4] {'tp'}, dimensions={1}, use_global_device_ids=true | all-gather | bytes 40960 | tf_op jit(solution)/shard_map/all_gather | solution.py:56
  13.8 0.7 fusion.10
  14.4 1.8 fusion.19
  16.2 1.8 fusion.17
  18.1 2.1 fusion.21
  20.2 0.7 mul.232
  21.0 21.2 %copy.77 = bf16[16,1024,2,128]{1,3,2,0:T(8,128)(2,1)} copy(bf16[16,1024,2,128]{3,2,1,0:T(2,128)(2,1)} %param.16) | data formatting | bytes 16777216 | tf_op args[1]
  42.1 14.4 %all-reduce.3.cloned.1.call-done = (f32[16,512]{1,0:T(8,128)}, f32[16]{0:T(128)}, f32[16,256]{1,0:T(8,128)}, f32[16,256]{1,0:T(8,128)}) async-done(((f32[16,512]{1,0:T(8,128)}, f32[16]{0:T(128)}, f32[16,256]{1,0:T(8,128)}, f32[16,256]{1,0:T(8,128)}), (f32[16,512]{1,0:T(8,128)}, f32[16]{0:T(128)}, f32[16,256]{1,0:T(8,128)}, f32[16,256]{1,0:T(8,128)})) %all-reduce.3.cloned.1.call-update) | async-done | bytes 65616 | tf_op jit(solution)/shard_map/psum | solution.py:62
  56.5 0.7 add_rsqrt_fusion.2
  57.2 0.8 multiply_convert_fusion.2
  58.0 0.8 fusion.29
  59.0 0.2 fusion.23
  59.3 4.7 %fusion.35 = (f32[16,2,2,2]{2,3,1,0:T(2,128)S(1)}, f32[16,2,2,2,1024]{4,2,3,1,0:T(2,128)S(1)}) fusion(bf16[16,1024,2,2,64]{1,4,3,2,0:T(8,128)(2,1)} %bitcast.56, bf16[16,2,2,2,64]{4,3,2,1,0:T(2,128)(2,1)S(1)} %reshape.43), kind=kOutput, calls=%fused_computation.55 | convolution fusion | flops 17039232 | bytes 8929792 | tf_op jit(solution)/shard_map/bkgch,bpkch->bkgcp/dot_general | solution.py:69
  64.1 0.3 copy.79
  64.4 0.5 fusion.7
  64.9 4.8 %fusion.3 = f32[16,2,2,2,128]{4,2,3,1,0:T(2,128)S(1)} fusion(bf16[16,1024,2,128,1]{3,2,1,0,4:T(2,128)(2,1)} %bitcast.65, f32[16,2,2,2,1024]{4,2,3,1,0:T(2,128)S(1)} %get-tuple-element.245, f32[16,2,2,2]{2,3,1,0:T(2,128)S(1)} %get-tuple-element.244), kind=kOutput, calls=%fused_computation.8 | convolution fusion | flops 33816576 | bytes 8978944 | tf_op jit(solution)/shard_map/bkgcp,bpkv->bkgcv/dot_general | solution.py:73
  69.7 0.3 copy.80
  70.0 13.6 %all-gather.1 = f32[64,2,2,2]{3,2,1,0:T(2,128)S(1)} all-gather(f32[16,2,2,2]{3,2,1,0:T(2,128)S(1)} %copy.80), channel_id=3, replica_groups=mesh['grp'=2,'kv'=4,'tp'=4] {'kv'}, dimensions={0}, use_global_device_ids=true | all-gather | bytes 2560 | tf_op jit(solution)/shard_map/all_gather | solution.py:15
  83.6 0.2 copy.88
  83.9 13.5 %all-gather = f32[64,2,2,2]{3,2,1,0:T(2,128)S(1)} all-gather(f32[16,2,2,2]{3,2,1,0:T(2,128)S(1)} %copy.79), channel_id=2, replica_groups=mesh['grp'=2,'kv'=4,'tp'=4] {'kv'}, dimensions={0}, use_global_device_ids=true | all-gather | bytes 2560 | tf_op jit(solution)/shard_map/all_gather | solution.py:15
  97.3 0.2 copy.87
  97.6 13.8 %all-gather.2 = f32[64,2,2,2,128]{4,3,2,1,0:T(2,128)S(1)} all-gather(f32[16,2,2,2,128]{4,3,2,1,0:T(2,128)S(1)} %copy.82), channel_id=4, replica_groups=mesh['grp'=2,'kv'=4,'tp'=4] {'kv'}, dimensions={0}, use_global_device_ids=true | all-gather | bytes 327680 | tf_op jit(solution)/shard_map/all_gather | solution.py:15
  111.4 2.1 while.19
  111.4 0.1 copy.115
  111.5 0.1 copy.116
  111.6 0.4 fusion.49
  112.1 0.1 copy.115
  112.3 0.4 fusion.49
  112.8 0.1 copy.115
  113.0 0.4 fusion.49
  113.5 0.1 copy.91
  113.8 0.3 add_divide_fusion
  114.1 0.1 slice_reduce_fusion
  114.3 0.2 multiply_reduce_fusion
  114.9 0.9 fusion.26
  115.9 19.9 %reduce-scatter.4.cloned.1.call-done = f32[16,256]{1,0:T(8,128)} async-done(((f32[16,1024]{1,0:T(8,128)}), f32[16,256]{1,0:T(8,128)}) %reduce-scatter.4.cloned.1.call-update) | async-done | bytes 16400 | tf_op jit(solution)/shard_map/reduce_scatter | solution.py:94
  135.8 0.7 add_convert_fusion.1
  136.5 5.2 %all_gather.34 = bf16[16,1024]{1,0:T(8,128)(2,1)S(1)} all-gather(bf16[16,256]{1,0:T(8,128)(2,1)S(1)} %add_convert_fusion.1), channel_id=1, replica_groups=mesh['grp'=2,'kv'=4,'tp'=4] {'tp'}, dimensions={1}, use_global_device_ids=true | all-gather | bytes 40960 | tf_op jit(solution)/shard_map/all_gather | solution.py:96
  141.7 5.3 %fusion.14 = f32[16,4096]{1,0:T(8,128)} fusion(bf16[1024,4096]{1,0:T(8,128)(2,1)} %param.26, bf16[16,1024]{1,0:T(8,128)(2,1)S(1)} %all_gather.34, f32[1024]{0:T(1024)S(1)} %convert_element_type.77), kind=kOutput, calls=%fused_computation.26 | convolution fusion | flops 134266880 | bytes 8687616 | tf_op jit(solution)/shard_map/dot_general | solution.py:98
  147.1 0.1 fusion.12
  147.2 11.8 %psum.39 = f32[16]{0:T(128)S(1)} all-reduce(f32[16]{0:T(128)S(1)} %fusion.12), channel_id=1, replica_groups=mesh['grp'=2,'kv'=4,'tp'=4] {'kv'}, use_global_device_ids=true, to_apply=%region_12.0 | all-reduce | flops 16 | bytes 128 | tf_op jit(solution)/shard_map/psum | solution.py:101
  159.0 8.2 %reduce-scatter.6.cloned.1.call-done = f32[16,1024]{1,0:T(8,128)} async-done(((f32[16,4096]{1,0:T(8,128)}), f32[16,1024]{1,0:T(8,128)}) %reduce-scatter.6.cloned.1.call-update) | async-done | bytes 65552 | tf_op jit(solution)/shard_map/reduce_scatter | solution.py:100
  167.2 0.9 multiply_convert_fusion
  168.1 13.4 %all_gather.35 = bf16[16,4096]{1,0:T(8,128)(2,1)S(1)} all-gather(bf16[16,1024]{1,0:T(8,128)(2,1)S(1)} %multiply_convert_fusion), channel_id=1, replica_groups=mesh['grp'=2,'kv'=4,'tp'=4] {'kv'}, dimensions={1}, use_global_device_ids=true | all-gather | bytes 163840 | tf_op jit(solution)/shard_map/all_gather | solution.py:104
  181.5 5.2 %fusion.36 = f32[16,1024]{1,0:T(8,128)} fusion(bf16[16,4096]{1,0:T(8,128)(2,1)S(1)} %all_gather.35, bf16[4096,1024]{1,0:T(8,128)(2,1)} %param.27), kind=kOutput, calls=%fused_computation.56 | convolution fusion | flops 134217728 | bytes 8585216 | tf_op jit(solution)/shard_map/dot_general | solution.py:105
  186.7 18.0 %reduce-scatter.8.cloned.1.call-done = f32[16,256]{1,0:T(8,128)} async-done(((f32[16,1024]{1,0:T(8,128)}), f32[16,256]{1,0:T(8,128)}) %reduce-scatter.8.cloned.1.call-update) | async-done | bytes 16400 | tf_op jit(solution)/shard_map/reduce_scatter | solution.py:107
  204.7 1.3 add_convert_fusion
  (45 shorter events, 1.8 us)
Async XLA Ops:
  6.5 108.4 %copy-start = (bf16[512,1024]{1,0:T(8,128)(2,1)S(1)}, bf16[512,1024]{1,0:T(8,128)(2,1)}, u32[]{:S(2)}) copy-start(bf16[512,1024]{1,0:T(8,128)(2,1)} %param.24) | copy-start | bytes 3145732
  6.5 50.0 %all-reduce.3.cloned.1.call-start = ((), (), s32[]{:S(2)}) async-start(), calls=%async_computation.6 | async-start | bytes 132096 | tf_op jit(solution)/shard_map/psum | solution.py:62
  20.2 115.6 %reduce-scatter.4.cloned.1.call-start = ((), (), s32[]{:S(2)}) async-start(), calls=%async_computation.3 | async-start | bytes 81920 | tf_op jit(solution)/shard_map/reduce_scatter | solution.py:94
  64.0 50.9 %copy-start.3 = (bf16[128]{0:T(256)(128)(2,1)S(1)}, bf16[128]{0:T(256)(128)(2,1)}, u32[]{:S(2)}) copy-start(bf16[128]{0:T(256)(128)(2,1)} %param.23) | copy-start | bytes 772
  64.0 51.8 %copy-start.2 = (bf16[1024]{0:T(1024)(128)(2,1)S(1)}, bf16[1024]{0:T(1024)(128)(2,1)}, u32[]{:S(2)}) copy-start(bf16[1024]{0:T(1024)(128)(2,1)} %param.25) | copy-start | bytes 6148
  64.1 71.8 %copy-start.1 = (bf16[16,256]{1,0:T(8,128)(2,1)S(1)}, bf16[16,256]{1,0:T(8,128)(2,1)}, u32[]{:S(2)}) copy-start(bf16[16,256]{1,0:T(8,128)(2,1)} %param.15) | copy-start | bytes 24580
  115.8 51.3 %reduce-scatter.6.cloned.1.call-start = ((), (), s32[]{:S(2)}) async-start(), calls=%async_computation.4 | async-start | bytes 327680 | tf_op jit(solution)/shard_map/reduce_scatter | solution.py:100
  147.0 57.6 %reduce-scatter.8.cloned.1.call-start = ((), (), s32[]{:S(2)}) async-start(), calls=%async_computation.5 | async-start | bytes 81920 | tf_op jit(solution)/shard_map/reduce_scatter | solution.py:107
Sparse Core Ops, SparseCore 0:
  20.3 36.1 all-reduce.2
  115.9 19.8 reduce-scatter.3
  147.1 19.9 reduce-scatter.5
  186.8 17.8 reduce-scatter.7
where the time goes:
time: 214 us; the launch traced here: 213 us
  blocking collectives  77.6 us (36%)
  waiting for transfers between devices  60.5 us (28%)
  matrix products  26.7 us (12%)
  local copies, waits for them, and re-layouts  25 us (12%)
  between operations  13.3 us (6%)
  other arithmetic  9.24 us (4%)
    all_gather x3, blocking collectives, joined(): everything = jax.tree.map(lambda part: lax.all_gather(part, axis), shard)  40.8 us
    unnamed x9, local copies, waits for them, and re-layouts  21.2 us
    reduce_scatter x1, waiting for transfers between devices, body(): lax.psum_scatter(projected, 'tp', scatter_dimension=1, tiled=True)  19.9 us
    reduce_scatter x1, waiting for transfers between devices, body(): lax.psum_scatter(down_part, 'tp', scatter_dimension=1, tiled=True)  18 us
    psum x1, waiting for transfers between devices, body(): lax.psum((q_part, k_part, v_part, sq_part), 'kv')  14.4 us
    all_gather x1, blocking collectives, body(): hidden = lax.all_gather(share, 'kv', axis=1, tiled=True)  13.4 us
    psum x1, blocking collectives, body(): sq_total = lax.psum(sq_mixed, 'kv')  11.8 us
    reduce_scatter x1, waiting for transfers between devices, body(): up_share = lax.psum_scatter(up_part, 'kv', scatter_dimension=1, tiled=True)  8.16 us
  transfers between devices with their start and end apart: 4, of which 4 were waited for; matrix products, arithmetic and copies ran while one was open for 10% of the time, Pallas kernels for 0%

commit v1 on v0

--- a/solution.py
+++ b/solution.py
@@ -101,7 +101,9 @@
     sq_total = lax.psum(sq_mixed, "kv")
     inv_rms2 = lax.rsqrt(sq_total / D + EPS)[:, None]
     share = jnp.square(jnp.maximum(inv_rms2 * up_share, 0.0)).astype(bf16)
-    hidden = lax.all_gather(share, "kv", axis=1, tiled=True)
+    hidden = jnp.concatenate(
+        lax.all_to_all(jnp.stack([share for _ in range(lax.psum(1, "kv"))]), "kv", 0, 0), axis=1
+    )
     down_part = jnp.dot(hidden, down_weight, preferred_element_type=f32)
     return (
         mixed.astype(f32) + lax.psum_scatter(down_part, "tp", scatter_dimension=1, tiled=True)

time: 214 us -> 210 us (0.981)
  blocking collectives: 77.6 us -> 72.5 us
    all_gather x1 -> x0, blocking collectives: 13.4 us -> none  [body(): hidden = lax.all_gather(share, 'kv', axis=1, tiled=True)]
    all_to_all x0 -> x1, blocking collectives: none -> 8.31 us  [body(): lax.all_to_all(jnp.stack([share for _ in range(lax.psum(1, 'kv'))]), 'kv'...]
  transfers between devices with their start and end apart: 4 -> 4, of which waited for: 4 -> 4; matrix products, arithmetic and copies ran while one was open for 10% -> 11% of each run, Pallas kernels for 0% -> 0%
where the time goes in v1:
time: 210 us; the launch traced here: 208 us
  blocking collectives  72.5 us (35%)
  waiting for transfers between devices  61.3 us (29%)
  matrix products  26.7 us (13%)
  local copies, waits for them, and re-layouts  25 us (12%)
  between operations  13.3 us (6%)
  other arithmetic  9.24 us (4%)
    all_gather x3, blocking collectives, joined(): everything = jax.tree.map(lambda part: lax.all_gather(part, axis), shard)  40.8 us
    unnamed x9, local copies, waits for them, and re-layouts  21.2 us
    reduce_scatter x1, waiting for transfers between devices, body(): lax.psum_scatter(projected, 'tp', scatter_dimension=1, tiled=True)  19.9 us
    reduce_scatter x1, waiting for transfers between devices, body(): lax.psum_scatter(down_part, 'tp', scatter_dimension=1, tiled=True)  18.7 us
    psum x1, waiting for transfers between devices, body(): lax.psum((q_part, k_part, v_part, sq_part), 'kv')  14.4 us
    psum x1, blocking collectives, body(): sq_total = lax.psum(sq_mixed, 'kv')  11.8 us
    all_to_all x1, blocking collectives, body(): lax.all_to_all(jnp.stack([share for _ in range(lax.psum(1, 'kv'))]), 'kv'...  8.31 us
    reduce_scatter x1, waiting for transfers between devices, body(): up_share = lax.psum_scatter(up_part, 'kv', scatter_dimension=1, tiled=True)  8.16 us
  transfers between devices with their start and end apart: 4, of which 4 were waited for; matrix products, arithmetic and copies ran while one was open for 11% of the time, Pallas kernels for 0%

profile of v1, /device:TPU:0, one launch (start us, length us, event | category | flops | bytes accessed | tf_op | source)
XLA Modules:
  0.0 208.2 jit_solution(15791653069957294733)
XLA Ops:
  6.5 0.8 convert_element_type.64
  7.3 6.4 %all_gather.24 = bf16[16,1024]{1,0:T(8,128)(2,1)S(1)} all-gather(bf16[16,256]{1,0:T(8,128)(2,1)} %param.15), channel_id=1, replica_groups=mesh['grp'=2,'kv'=4,'tp'=4] {'tp'}, dimensions={1}, use_global_device_ids=true | all-gather | bytes 40960 | tf_op jit(solution)/shard_map/all_gather | solution.py:56
  13.8 0.7 fusion.10
  14.4 1.8 fusion.19
  16.2 1.8 fusion.17
  18.1 2.1 %fusion.21 = f32[16,512]{1,0:T(8,128)} fusion(bf16[1024,512]{1,0:T(8,128)(2,1)} %param.19, bf16[16,1024]{1,0:T(8,128)(2,1)S(1)} %all_gather.24, f32[1024]{0:T(1024)S(1)} %convert_element_type.64), kind=kOutput, calls=%fused_computation.33 | convolution fusion | flops 16826368 | bytes 1118208 | tf_op jit(solution)/shard_map/dot_general | solution.py:58
  20.2 0.7 mul.232
  21.0 21.2 %copy.79 = bf16[16,1024,2,128]{1,3,2,0:T(8,128)(2,1)} copy(bf16[16,1024,2,128]{3,2,1,0:T(2,128)(2,1)} %param.16) | data formatting | bytes 16777216 | tf_op args[1]
  42.1 14.4 %all-reduce.3.cloned.1.call-done = (f32[16,512]{1,0:T(8,128)}, f32[16]{0:T(128)}, f32[16,256]{1,0:T(8,128)}, f32[16,256]{1,0:T(8,128)}) async-done(((f32[16,512]{1,0:T(8,128)}, f32[16]{0:T(128)}, f32[16,256]{1,0:T(8,128)}, f32[16,256]{1,0:T(8,128)}), (f32[16,512]{1,0:T(8,128)}, f32[16]{0:T(128)}, f32[16,256]{1,0:T(8,128)}, f32[16,256]{1,0:T(8,128)})) %all-reduce.3.cloned.1.call-update) | async-done | bytes 65616 | tf_op jit(solution)/shard_map/psum | solution.py:62
  56.5 0.7 add_rsqrt_fusion.2
  57.2 0.8 multiply_convert_fusion.2
  58.0 0.8 fusion.29
  59.0 0.2 fusion.23
  59.3 4.7 %fusion.35 = (f32[16,2,2,2]{2,3,1,0:T(2,128)S(1)}, f32[16,2,2,2,1024]{4,2,3,1,0:T(2,128)S(1)}) fusion(bf16[16,1024,2,2,64]{1,4,3,2,0:T(8,128)(2,1)} %bitcast.59, bf16[16,2,2,2,64]{4,3,2,1,0:T(2,128)(2,1)S(1)} %reshape.51), kind=kOutput, calls=%fused_computation.55 | convolution fusion | flops 17039232 | bytes 8929792 | tf_op jit(solution)/shard_map/bkgch,bpkch->bkgcp/dot_general | solution.py:69
  64.1 0.3 copy.81
  64.4 0.5 fusion.7
  64.9 4.8 %fusion.3 = f32[16,2,2,2,128]{4,2,3,1,0:T(2,128)S(1)} fusion(bf16[16,1024,2,128,1]{3,2,1,0,4:T(2,128)(2,1)} %bitcast.70, f32[16,2,2,2,1024]{4,2,3,1,0:T(2,128)S(1)} %get-tuple-element.245, f32[16,2,2,2]{2,3,1,0:T(2,128)S(1)} %get-tuple-element.244), kind=kOutput, calls=%fused_computation.8 | convolution fusion | flops 33816576 | bytes 8978944 | tf_op jit(solution)/shard_map/bkgcp,bpkv->bkgcv/dot_general | solution.py:73
  69.7 0.3 copy.82
  70.0 13.6 %all-gather.1 = f32[64,2,2,2]{3,2,1,0:T(2,128)S(1)} all-gather(f32[16,2,2,2]{3,2,1,0:T(2,128)S(1)} %copy.82), channel_id=3, replica_groups=mesh['grp'=2,'kv'=4,'tp'=4] {'kv'}, dimensions={0}, use_global_device_ids=true | all-gather | bytes 2560 | tf_op jit(solution)/shard_map/all_gather | solution.py:15
  83.6 0.2 copy.90
  83.9 13.5 %all-gather = f32[64,2,2,2]{3,2,1,0:T(2,128)S(1)} all-gather(f32[16,2,2,2]{3,2,1,0:T(2,128)S(1)} %copy.81), channel_id=2, replica_groups=mesh['grp'=2,'kv'=4,'tp'=4] {'kv'}, dimensions={0}, use_global_device_ids=true | all-gather | bytes 2560 | tf_op jit(solution)/shard_map/all_gather | solution.py:15
  97.3 0.2 copy.89
  97.6 13.8 %all-gather.2 = f32[64,2,2,2,128]{4,3,2,1,0:T(2,128)S(1)} all-gather(f32[16,2,2,2,128]{4,3,2,1,0:T(2,128)S(1)} %copy.84), channel_id=4, replica_groups=mesh['grp'=2,'kv'=4,'tp'=4] {'kv'}, dimensions={0}, use_global_device_ids=true | all-gather | bytes 327680 | tf_op jit(solution)/shard_map/all_gather | solution.py:15
  111.4 2.1 while.19
  111.4 0.1 copy.119
  111.5 0.1 copy.120
  111.6 0.4 fusion.49
  112.1 0.1 copy.119
  112.3 0.4 fusion.49
  112.8 0.1 copy.119
  113.0 0.4 fusion.49
  113.5 0.1 copy.93
  113.8 0.3 add_divide_fusion
  114.1 0.1 slice_reduce_fusion
  114.3 0.2 multiply_reduce_fusion
  114.9 0.9 fusion.26
  115.9 19.9 %reduce-scatter.4.cloned.1.call-done = f32[16,256]{1,0:T(8,128)} async-done(((f32[16,1024]{1,0:T(8,128)}), f32[16,256]{1,0:T(8,128)}) %reduce-scatter.4.cloned.1.call-update) | async-done | bytes 16400 | tf_op jit(solution)/shard_map/reduce_scatter | solution.py:94
  135.8 0.7 add_convert_fusion.1
  136.5 5.2 %all_gather.31 = bf16[16,1024]{1,0:T(8,128)(2,1)S(1)} all-gather(bf16[16,256]{1,0:T(8,128)(2,1)S(1)} %add_convert_fusion.1), channel_id=1, replica_groups=mesh['grp'=2,'kv'=4,'tp'=4] {'tp'}, dimensions={1}, use_global_device_ids=true | all-gather | bytes 40960 | tf_op jit(solution)/shard_map/all_gather | solution.py:96
  141.7 5.3 %fusion.14 = f32[16,4096]{1,0:T(8,128)} fusion(bf16[1024,4096]{1,0:T(8,128)(2,1)} %param.26, bf16[16,1024]{1,0:T(8,128)(2,1)S(1)} %all_gather.31, f32[1024]{0:T(1024)S(1)} %convert_element_type.77), kind=kOutput, calls=%fused_computation.26 | convolution fusion | flops 134266880 | bytes 8687616 | tf_op jit(solution)/shard_map/dot_general | solution.py:98
  147.1 0.1 fusion.12
  147.2 11.8 %psum.39 = f32[16]{0:T(128)S(1)} all-reduce(f32[16]{0:T(128)S(1)} %fusion.12), channel_id=1, replica_groups=mesh['grp'=2,'kv'=4,'tp'=4] {'kv'}, use_global_device_ids=true, to_apply=%region_12.0 | all-reduce | flops 16 | bytes 128 | tf_op jit(solution)/shard_map/psum | solution.py:101
  159.0 8.2 %reduce-scatter.6.cloned.1.call-done = f32[16,1024]{1,0:T(8,128)} async-done(((f32[16,4096]{1,0:T(8,128)}), f32[16,1024]{1,0:T(8,128)}) %reduce-scatter.6.cloned.1.call-update) | async-done | bytes 65552 | tf_op jit(solution)/shard_map/reduce_scatter | solution.py:100
  167.2 0.9 multiply_convert_fusion
  168.1 8.3 %all_to_all.5 = bf16[4,16,1024]{2,1,0:T(8,128)(2,1)S(1)} all-to-all(bf16[4,16,1024]{2,1,0:T(8,128)(2,1)S(1)} %stack.2), channel_id=1, replica_groups=mesh['grp'=2,'kv'=4,'tp'=4] {'kv'}, dimensions={0} | all-to-all | bytes 262144 | tf_op jit(solution)/shard_map/all_to_all | solution.py:105
  176.4 5.2 %fusion.36 = f32[16,1024]{1,0:T(8,128)} fusion(bf16[16,4096]{1,0:T(8,128)(2,1)S(1)} %bitcast.61, bf16[4096,1024]{1,0:T(8,128)(2,1)} %param.27), kind=kOutput, calls=%fused_computation.56 | convolution fusion | flops 134217728 | bytes 8585216 | tf_op jit(solution)/shard_map/dot_general | solution.py:107
  181.6 18.7 %reduce-scatter.8.cloned.1.call-done = f32[16,256]{1,0:T(8,128)} async-done(((f32[16,1024]{1,0:T(8,128)}), f32[16,256]{1,0:T(8,128)}) %reduce-scatter.8.cloned.1.call-update) | async-done | bytes 16400 | tf_op jit(solution)/shard_map/reduce_scatter | solution.py:109
  200.4 1.3 add_convert_fusion
  (47 shorter events, 1.8 us)
Async XLA Ops:
  6.5 108.4 %copy-start = (bf16[512,1024]{1,0:T(8,128)(2,1)S(1)}, bf16[512,1024]{1,0:T(8,128)(2,1)}, u32[]{:S(2)}) copy-start(bf16[512,1024]{1,0:T(8,128)(2,1)} %param.24) | copy-start | bytes 3145732
  6.5 50.0 %all-reduce.3.cloned.1.call-start = ((), (), s32[]{:S(2)}) async-start(), calls=%async_computation.7 | async-start | bytes 132096 | tf_op jit(solution)/shard_map/psum | solution.py:62
  20.2 115.6 %reduce-scatter.4.cloned.1.call-start = ((), (), s32[]{:S(2)}) async-start(), calls=%async_computation.4 | async-start | bytes 81920 | tf_op jit(solution)/shard_map/reduce_scatter | solution.py:94
  64.0 50.9 %copy-start.3 = (bf16[128]{0:T(256)(128)(2,1)S(1)}, bf16[128]{0:T(256)(128)(2,1)}, u32[]{:S(2)}) copy-start(bf16[128]{0:T(256)(128)(2,1)} %param.23) | copy-start | bytes 772
  64.0 51.8 %copy-start.2 = (bf16[1024]{0:T(1024)(128)(2,1)S(1)}, bf16[1024]{0:T(1024)(128)(2,1)}, u32[]{:S(2)}) copy-start(bf16[1024]{0:T(1024)(128)(2,1)} %param.25) | copy-start | bytes 6148
  64.1 71.8 %copy-start.1 = (bf16[16,256]{1,0:T(8,128)(2,1)S(1)}, bf16[16,256]{1,0:T(8,128)(2,1)}, u32[]{:S(2)}) copy-start(bf16[16,256]{1,0:T(8,128)(2,1)} %param.15) | copy-start | bytes 24580
  115.8 51.3 %reduce-scatter.6.cloned.1.call-start = ((), (), s32[]{:S(2)}) async-start(), calls=%async_computation.5 | async-start | bytes 327680 | tf_op jit(solution)/shard_map/reduce_scatter | solution.py:100
  147.0 53.4 %reduce-scatter.8.cloned.1.call-start = ((), (), s32[]{:S(2)}) async-start(), calls=%async_computation.6 | async-start | bytes 81920 | tf_op jit(solution)/shard_map/reduce_scatter | solution.py:109
Sparse Core Ops, SparseCore 0:
  20.3 36.1 all-reduce.2
  115.9 19.8 reduce-scatter.3
  147.1 19.9 reduce-scatter.5
  181.8 18.5 reduce-scatter.7
